TPU v7x, 32 devices: a whole 2x2x4 slice. The times are simulated.
32 devices in a mesh: sp: 4 (over z), fs: 4 (over y, x), tp: 2 (over core).
Axes of the slice: x: 2, y: 2, z: 4, core: 2. Of those that a mesh axis runs over, the one named last changes fastest.
Arguments:
- tokens: bfloat16 [4, 2048, 2048], P('fs', ('sp', 'tp')), may hold values from -6 to 6
- norm_gain: float32 [2048], replicated, may hold values from 0.1 to 1.9
- query_weight: bfloat16 [2048, 1024], P('sp', 'tp'), may hold values from -20 to 20
- key_matrix: bfloat16 [2048, 256], P('sp', 'tp'), may hold values from -0.125 to 0.125
- value_matrix: bfloat16 [2048, 256], P('sp', 'tp'), may hold values from -0.125 to 0.125
- pool_in_weight: bfloat16 [2048, 1024], P('sp', 'tp'), may hold values from -0.125 to 0.125
- head_sink_logit: float32 [16], replicated, may hold values from 2 to 6
- pool_mix: bfloat16 [4, 256, 256], replicated, may hold values from -0.375 to 0.375
- pool_gain: float32 [1024], replicated, may hold values from 0.1 to 1.9
- attn_out_weight: bfloat16 [1024, 2048], P('tp', 'sp'), may hold values from -1 to 1
- pool_out_weight: bfloat16 [1024, 2048], P('tp', 'sp'), may hold values from -0.125 to 0.125
Outputs:
- mixed: bfloat16 [4, 2048, 2048], P('fs', ('sp', 'tp'))
- row_log_weight_sum: float32 [4, 16, 2048], P('fs', 'tp', 'sp')
All inputs are finite; a program needn't handle non-finite values.
Results may differ from a plain program's by a relative error of at most 0.0095.
The roundings to bfloat16 on the way count: a program that leaves them out, or rounds other values in their place, can miss the bound.
Values may be sent and summed in bfloat16 or wider, within the bound.
No kernel may reach another device: no remote copies, remote signals or barrier semaphores. Data moves between devices by JAX's collectives and lax.ppermute only.
A program may use at most 64 MiB of HBM per device.

v0:
```python
import jax
import jax.numpy as jnp
from jax import lax
from jax.sharding import PartitionSpec as P

HEAD_SIZE = 64
WINDOW = 128
POOL_CH = 256
EPSILON = 1e-06
POOL_SPANS = (2, 4, 8, 16)


def passed_along(shard, axis, by):
    size = lax.axis_size(axis)
    pairs = [(i, i + by) for i in range(size) if 0 <= i + by < size]
    return lax.ppermute(shard, axis, pairs)


def windowed_attend(
    query_rows, key_rows, value_rows, key_tail, value_tail, sinks, kv_heads, group, first_pos
):
    rows = query_rows.shape[0]
    blocks = rows // WINDOW
    width = key_rows.shape[1]
    ext_keys = jnp.concatenate([key_tail, key_rows], 0)
    ext_values = jnp.concatenate([value_tail, value_rows], 0)

    def banded(table):
        return jnp.concatenate(
            [
                table[:rows].reshape(blocks, WINDOW, width),
                table[WINDOW:].reshape(blocks, WINDOW, width),
            ],
            axis=1,
        )

    band_keys = banded(ext_keys).reshape(blocks, 2 * WINDOW, kv_heads, HEAD_SIZE)
    band_values = banded(ext_values).reshape(blocks, 2 * WINDOW, kv_heads, HEAD_SIZE)
    query_blocks = query_rows.reshape(blocks, WINDOW, kv_heads, group, HEAD_SIZE)
    scores = jnp.einsum(
        "bqkgd,bskd->bkgqs", query_blocks, band_keys, preferred_element_type=jnp.float32
    ) * HEAD_SIZE ** (-0.5)
    query_pos = first_pos + jnp.arange(rows).reshape(blocks, WINDOW, 1)
    key_pos = (
        first_pos
        - WINDOW
        + jnp.arange(blocks).reshape(blocks, 1, 1) * WINDOW
        + jnp.arange(2 * WINDOW).reshape(1, 1, 2 * WINDOW)
    )
    offset = query_pos - key_pos
    allowed = (offset >= 0) & (offset < WINDOW) & (key_pos >= 0)
    scores = jnp.where(allowed[:, None, None], scores, -jnp.inf)
    sink_grid = sinks.reshape(1, kv_heads, group, 1, 1)
    top = jnp.maximum(jnp.max(scores, axis=-1, keepdims=True), sink_grid)
    weights = jnp.exp(scores - top)
    total = jnp.sum(weights, axis=-1, keepdims=True) + jnp.exp(sink_grid - top)
    probs = (weights / total).astype(jnp.bfloat16)
    mixed = jnp.einsum(
        "bkgqs,bskd->bqkgd", probs, band_values, preferred_element_type=jnp.float32
    ).astype(jnp.bfloat16)
    row_log_weight_sum = (top + jnp.log(total))[..., 0]
    return (
        mixed.reshape(rows, kv_heads * group * HEAD_SIZE),
        row_log_weight_sum.transpose(1, 2, 0, 3).reshape(kv_heads * group, rows),
    )


def pool_branch(pool_rows, pool_tail, mixing, scales, group_start, first_pos):
    rows = pool_rows.shape[0]
    columns = pool_rows.shape[1]
    pool_reach = max(POOL_SPANS)
    extended = jnp.concatenate([pool_tail, pool_rows], 0).astype(jnp.float32)
    group_index = group_start + jnp.arange(columns) // POOL_CH
    span_table = jnp.array(POOL_SPANS, jnp.int32)
    matches = group_index[:, None] == jnp.arange(len(POOL_SPANS))[None, :]
    span_of_col = jnp.sum(jnp.where(matches, span_table[None, :], 0), axis=1)
    trailing = jnp.zeros((rows, columns), jnp.float32)
    for lag in range(pool_reach):
        trailing = trailing + jnp.where(
            lag < span_of_col[None, :], extended[pool_reach - lag : pool_reach - lag + rows], 0.0
        )
    position = first_pos + jnp.arange(rows)
    count = jnp.minimum(position[:, None] + 1, span_of_col[None, :]).astype(jnp.float32)
    centred = (trailing / count - extended[pool_reach:]).astype(jnp.bfloat16)
    grouped = centred.reshape(rows, columns // POOL_CH, POOL_CH)
    product = jnp.einsum(
        "rgc,gcd->rgd", grouped, mixing, preferred_element_type=jnp.float32
    ).reshape(rows, columns)
    return (product * scales).astype(jnp.bfloat16)


def local(
    tokens,
    norm_gain,
    query_weight,
    key_matrix,
    value_matrix,
    pool_in_weight,
    head_sink_logit,
    pool_mix,
    pool_gain,
    attn_out_weight,
    pool_out_weight,
):
    tp_index = lax.axis_index("tp")
    sp_index = lax.axis_index("sp")
    q_cols = query_weight.shape[1]
    kv_cols = key_matrix.shape[1]
    pool_cols = pool_in_weight.shape[1]
    q_heads = q_cols // HEAD_SIZE
    kv_heads = kv_cols // HEAD_SIZE
    groups_dev = pool_cols // POOL_CH
    full_query, full_key, full_value, full_pool = (
        lax.all_gather(query_weight, "sp", axis=0, tiled=True),
        lax.all_gather(key_matrix, "sp", axis=0, tiled=True),
        lax.all_gather(value_matrix, "sp", axis=0, tiled=True),
        lax.all_gather(pool_in_weight, "sp", axis=0, tiled=True),
    )
    values_f = lax.all_gather(tokens[0], "tp", axis=0, tiled=True).astype(jnp.float32)
    scale = lax.rsqrt(jnp.mean(values_f * values_f, axis=-1, keepdims=True) + EPSILON)
    normed = (values_f * scale * norm_gain).astype(jnp.bfloat16)
    outputs = [
        jnp.dot(normed, weight, preferred_element_type=jnp.float32).astype(jnp.bfloat16)
        for weight in (full_query, full_key, full_value, full_pool)
    ]
    projected = jnp.concatenate(outputs, axis=1)
    rows = projected.shape[0]
    first_pos = sp_index * rows
    query_rows = projected[:, :q_cols]
    key_rows = projected[:, q_cols : q_cols + kv_cols]
    value_rows = projected[:, q_cols + kv_cols : q_cols + 2 * kv_cols]
    pool_rows = projected[:, q_cols + 2 * kv_cols :]
    pool_reach = max(POOL_SPANS)
    sinks = lax.dynamic_slice_in_dim(head_sink_logit, tp_index * q_heads, q_heads, 0)
    mixing = lax.dynamic_slice_in_dim(pool_mix, tp_index * groups_dev, groups_dev, 0)
    scales = lax.dynamic_slice_in_dim(pool_gain, tp_index * pool_cols, pool_cols, 0)
    key_tail, value_tail, pool_tail = passed_along(
        (key_rows[rows - WINDOW :], value_rows[rows - WINDOW :], pool_rows[rows - pool_reach :]),
        "sp",
        1,
    )
    attn_part, log_part = windowed_attend(
        query_rows,
        key_rows,
        value_rows,
        key_tail,
        value_tail,
        sinks,
        kv_heads,
        q_heads // kv_heads,
        first_pos,
    )
    pool_part = pool_branch(pool_rows, pool_tail, mixing, scales, tp_index * groups_dev, first_pos)
    half_attn, half_pool = (
        lax.all_gather(attn_out_weight, "sp", axis=1, tiled=True),
        lax.all_gather(pool_out_weight, "sp", axis=1, tiled=True),
    )
    result = lax.psum_scatter(
        jnp.dot(attn_part, half_attn, preferred_element_type=jnp.float32)
        + jnp.dot(pool_part, half_pool, preferred_element_type=jnp.float32),
        "tp",
        scatter_dimension=0,
        tiled=True,
    ).astype(jnp.bfloat16)
    return (result[None], log_part[None])


def solution(mesh):
    in_specs = (
        P("fs", ("sp", "tp"), None),
        P(),
        P("sp", "tp"),
        P("sp", "tp"),
        P("sp", "tp"),
        P("sp", "tp"),
        P(),
        P(),
        P(),
        P("tp", "sp"),
        P("tp", "sp"),
    )
    out_specs = (P("fs", ("sp", "tp"), None), P("fs", "tp", "sp"))
    return jax.shard_map(local, mesh=mesh, in_specs=in_specs, out_specs=out_specs, check_vma=False)
```

profile of v0, /device:TPU:0, one launch (start us, length us, event | category | flops | bytes accessed | tf_op | source)
XLA Modules:
  0.0 243.1 jit_solution(15689682092924149541)
XLA Ops:
  7.2 0.0 all-gather.15.cloned.1.call-start
  7.3 0.7 all-gather.15.cloned.1.call-update
  7.9 0.0 all-gather.7.cloned.1.call-start
  8.0 0.7 all-gather.7.cloned.1.call-update
  8.7 0.0 all-gather.11.cloned.1.call-start
  8.7 0.7 all-gather.11.cloned.1.call-update
  9.4 0.0 all-gather.9.cloned.1.call-start
  9.5 0.5 all-gather.9.cloned.1.call-update
  10.0 0.0 all-gather.13.cloned.1.call-start
  10.1 0.5 all-gather.13.cloned.1.call-update
  10.6 0.0 reduce-scatter.2.cloned.1.call-start
  10.7 0.1 iota_add_fusion
  10.7 0.1 broadcast_compare_fusion
  10.8 17.6 %all_gather.23 = bf16[2048,128]{1,0:T(8,128)(2,1)S(1)} all-gather(bf16[512,128]{1,0:T(8,128)(2,1)} %param.15), channel_id=1, replica_groups=mesh['sp'=4,'fs'=4,'tp'=2] {'sp'}, dimensions={0}, use_global_device_ids=true | all-gather | bytes 655360 | tf_op jit(solution)/shard_map/all_gather | solution.py:115
  28.4 0.7 dynamic_slice.9
  29.1 0.1 max.26
  29.2 23.4 %all_gather.22 = bf16[2048,128]{1,0:T(8,128)(2,1)} all-gather(bf16[512,128]{1,0:T(8,128)(2,1)} %param.16), channel_id=1, replica_groups=mesh['sp'=4,'fs'=4,'tp'=2] {'sp'}, dimensions={0}, use_global_device_ids=true | all-gather | bytes 655360 | tf_op jit(solution)/shard_map/all_gather | solution.py:116
  52.6 0.1 select_reduce_fusion
  52.7 0.6 broadcast_compare_fusion.15
  53.4 0.1 dynamic_slice.11
  53.5 0.3 fusion.36
  53.8 0.0 all-gather.15.cloned.1.call-done
  53.9 2.2 fusion
  56.1 2.4 convolution_convert_fusion.2
  58.5 0.6 slice.86
  59.1 3.5 %collective-permute-start.1 = (bf16[128,128]{1,0:T(8,128)(2,1)}, bf16[128,128]{1,0:T(8,128)(2,1)}, u32[]{:S(2)}, u32[]{:S(2)}) collective-permute-start(bf16[128,128]{1,0:T(8,128)(2,1)} %slice.86), channel_id=1, source_target_pairs={{0,8},{8,16},{16,24},{1,9},{9,17},{17,25},{2,10},{10,18},{18,26},{... | collective-permute-start | bytes 98312 | tf_op jit(solution)/shard_map/ppermute | solution.py:16
  62.6 1.5 convolution_convert_fusion.3
  64.1 0.1 reshape.235
  64.2 0.6 slice.85
  64.8 0.1 reshape.233
  65.0 0.8 copy.45
  65.8 2.0 collective-permute-start
  67.8 0.8 copy.41
  68.5 0.8 pad_maximum_fusion
  69.3 0.1 reshape.234
  69.5 0.8 copy.44
  70.3 0.1 collective-permute-done
  70.3 0.1 reshape.232
  70.5 0.8 copy.40
  71.3 5.5 %all-gather.7.cloned.1.call-done = bf16[2048,512]{1,0:T(8,128)(2,1)} async-done(((bf16[512,512]{1,0:T(8,128)(2,1)}), bf16[2048,512]{1,0:T(8,128)(2,1)}) %all-gather.7.cloned.1.call-update) | async-done | bytes 2097168 | tf_op jit(solution)/shard_map/all_gather | solution.py:114
  76.8 2.9 %convolution_convert_fusion.1 = bf16[512,512]{1,0:T(8,128)(2,1)S(1)} fusion(bf16[2048,512]{1,0:T(8,128)(2,1)} %all-gather.7.cloned.1.call-done, bf16[1,512,2048]{2,1,0:T(8,128)(2,1)S(1)} %copy-done.1, f32[2048]{0:T(1024)} %param.13, f32[512]{0:T(512)} %copy-done.23), kind=kOutput, calls=%fused_computation.13 | convolution fusion | flops 1078198272 | bytes 4728832 | tf_op jit(solution)/shard_map/dot_general | solution.py:123
  79.7 1.5 reshape.236
  81.3 2.3 fusion.4
  83.5 0.1 broadcast_maximum_fusion
  83.6 1.0 fusion.3
  84.6 0.1 exponential_add_fusion
  84.7 1.2 fusion.7
  85.9 0.4 copy.49
  86.3 38.3 %all-gather.11.cloned.1.call-done = bf16[2048,512]{1,0:T(8,128)(2,1)} async-done(((bf16[512,512]{1,0:T(8,128)(2,1)}), bf16[2048,512]{1,0:T(8,128)(2,1)}) %all-gather.11.cloned.1.call-update) | async-done | bytes 2097168 | tf_op jit(solution)/shard_map/all_gather | solution.py:117
  124.6 2.9 %convolution_convert_fusion = bf16[512,512]{1,0:T(8,128)(2,1)S(1)} fusion(bf16[2048,512]{1,0:T(8,128)(2,1)} %all-gather.11.cloned.1.call-done, bf16[1,512,2048]{2,1,0:T(8,128)(2,1)S(1)} %copy-done.1, f32[2048]{0:T(1024)S(1)} %copy-done.28, f32[512]{0:T(512)S(1)} %copy-done.24), kind=kOutput, calls=%fused_computation.12 | convolution fusion | flops 1078198272 | bytes 4728832 | tf_op jit(solution)/shard_map/dot_general | solution.py:123
  127.5 0.8 copy-done.2
  128.3 2.4 collective-permute-start.2
  130.7 39.8 %all-gather.9.cloned.1.call-done = bf16[512,2048]{1,0:T(8,128)(2,1)} async-done(((bf16[512,512]{1,0:T(8,128)(2,1)}), bf16[512,2048]{1,0:T(8,128)(2,1)}) %all-gather.9.cloned.1.call-update) | async-done | bytes 2097168 | tf_op jit(solution)/shard_map/all_gather | solution.py:155
  170.6 4.9 %fusion.29 = f32[512,2048]{1,0:T(8,128)} fusion(bf16[512,2048]{1,0:T(8,128)(2,1)} %all-gather.9.cloned.1.call-done, bf16[64,8,4,128]{3,2,1,0:T(4,128)(2,1)S(1)} %bitcast.76), kind=kOutput, calls=%fused_computation.59 | convolution fusion | flops 1073741824 | bytes 6815744 | tf_op jit(solution)/shard_map/dot_general | solution.py:159
  175.5 0.1 maximum_convert_fusion
  175.8 3.0 %fusion.28 = bf16[512,512]{1,0:T(8,128)(2,1)S(1)} fusion(f32[528,512]{1,0:T(8,128)S(1)} %maximum_convert_fusion, s32[512]{0:T(512)S(1)} %select_reduce_fusion, s32[512]{0:T(512)S(1)} %add_add_fusion, pred[512]{0:T(512)(128)(4,1)S(1)} %copy-done.8, pred[512]{0:T(512)(128)(4,1)S(1)} %copy-done.9, pred[512]{0:T(512)(128)(4,1)S(1)} %copy-done.10, ...), kind=kLoop, calls=%fused_computation.55 | loop fusion | flops 9437184 | bytes 17313792 | tf_op jit(solution)/shard_map/convert_element_type | solution.py:84
  178.8 0.4 fusion.32
  179.2 0.1 fusion.25
  179.3 37.1 %all-gather.13.cloned.1.call-done = bf16[512,2048]{1,0:T(8,128)(2,1)} async-done(((bf16[512,512]{1,0:T(8,128)(2,1)}), bf16[512,2048]{1,0:T(8,128)(2,1)}) %all-gather.13.cloned.1.call-update) | async-done | bytes 2097168 | tf_op jit(solution)/shard_map/all_gather | solution.py:156
  216.4 6.1 %convolution_add_fusion = f32[512,2048]{1,0:T(8,128)} fusion(f32[512,2048]{1,0:T(8,128)} %fusion.29, bf16[512,512]{0,1:T(8,128)(2,1)S(1)} %fusion.25, bf16[512,2048]{1,0:T(8,128)(2,1)} %all-gather.13.cloned.1.call-done), kind=kOutput, calls=%fused_computation.9 | convolution fusion | flops 1074790400 | bytes 11010048 | tf_op jit(solution)/shard_map/dot_general | solution.py:160
  222.5 0.0 reduce-scatter.2.cloned.1.call-update
  222.5 0.7 fusion.43
  223.2 10.3 %reduce-scatter.2.cloned.1.call-done = f32[256,2048]{1,0:T(8,128)} async-done(((f32[512,2048]{1,0:T(8,128)}), f32[256,2048]{1,0:T(8,128)}) %reduce-scatter.2.cloned.1.call-update) | async-done | bytes 2097168 | tf_op jit(solution)/shard_map/reduce_scatter | solution.py:158
  233.5 2.7 %convert_bitcast_fusion = bf16[1,256,2048]{2,1,0:T(8,128)(2,1)} fusion(f32[256,2048]{1,0:T(8,128)} %reduce-scatter.2.cloned.1.call-done), kind=kLoop, calls=%fused_computation.54 | loop fusion | flops 524288 | bytes 3145728 | tf_op jit(solution)/shard_map/broadcast_in_dim | solution.py:165
  (66 shorter events, 0.2 us)
Async XLA Ops:
  7.2 171.7 %copy-start = (bf16[4,256,256]{2,1,0:T(8,128)(2,1)S(1)}, bf16[4,256,256]{2,1,0:T(8,128)(2,1)}, u32[]{:S(2)}) copy-start(bf16[4,256,256]{2,1,0:T(8,128)(2,1)} %param.19) | copy-start | bytes 1572868
  7.2 45.5 %copy-start.26 = (s32[4]{0:T(128)S(1)}, s32[4]{0:T(128)}, u32[]{:S(2)}) copy-start(s32[4]{0:T(128)} %constant.89.clone) | copy-start | bytes 52
  7.2 46.2 %copy-start.25 = (f32[1024]{0:T(1024)S(1)}, f32[1024]{0:T(1024)}, u32[]{:S(2)}) copy-start(f32[1024]{0:T(1024)} %param.20) | copy-start | bytes 12292
  7.2 48.9 %copy-start.27 = (f32[2048]{0:T(1024)S(1)}, f32[2048]{0:T(1024)}, u32[]{:S(2)}) copy-start(f32[2048]{0:T(1024)} %param.13) | copy-start | bytes 24580
  7.2 46.6 %all-gather.15.cloned.1.call-start = ((), (), s32[]{:S(2)}) async-start(), calls=%async_computation.6 | async-start | bytes 3145728 | tf_op jit(solution)/shard_map/all_gather | solution.py:119
  7.9 68.9 %all-gather.7.cloned.1.call-start = ((), (), s32[]{:S(2)}) async-start(), calls=%async_computation.1 | async-start | bytes 2621440 | tf_op jit(solution)/shard_map/all_gather | solution.py:114
  8.7 115.9 %all-gather.11.cloned.1.call-start = ((), (), s32[]{:S(2)}) async-start(), calls=%async_computation.3 | async-start | bytes 2621440 | tf_op jit(solution)/shard_map/all_gather | solution.py:117
  9.4 161.1 %all-gather.9.cloned.1.call-start = ((), (), s32[]{:S(2)}) async-start(), calls=%async_computation.2 | async-start | bytes 2621440 | tf_op jit(solution)/shard_map/all_gather | solution.py:155
  10.0 206.4 %all-gather.13.cloned.1.call-start = ((), (), s32[]{:S(2)}) async-start(), calls=%async_computation.4 | async-start | bytes 2621440 | tf_op jit(solution)/shard_map/all_gather | solution.py:156
  10.6 222.9 %reduce-scatter.2.cloned.1.call-start = ((), (), s32[]{:S(2)}) async-start(), calls=%async_computation.5 | async-start | bytes 6291456 | tf_op jit(solution)/shard_map/reduce_scatter | solution.py:158
  53.8 8.8 %copy-start.1 = (bf16[1,512,2048]{2,1,0:T(8,128)(2,1)S(1)}, bf16[1,512,2048]{2,1,0:T(8,128)(2,1)}, u32[]{:S(2)}) copy-start(bf16[1,512,2048]{2,1,0:T(8,128)(2,1)} %all-gather.15.cloned.1.call-done) | copy-start | bytes 6291460
  53.8 8.8 %copy-start.4 = (bf16[2048,128]{1,0:T(8,128)(2,1)S(1)}, bf16[2048,128]{1,0:T(8,128)(2,1)}, u32[]{:S(2)}) copy-start(bf16[2048,128]{1,0:T(8,128)(2,1)} %all_gather.22) | copy-start | bytes 1572868
  56.1 6.5 %copy-start.23 = (f32[512]{0:T(512)}, f32[512]{0:T(512)S(1)}, u32[]{:S(2)}) copy-start(f32[512]{0:T(512)S(1)} %add_rsqrt_fusion) | copy-start | bytes 6148
  59.1 9.4 %collective-permute-start.1 = (bf16[128,128]{1,0:T(8,128)(2,1)}, bf16[128,128]{1,0:T(8,128)(2,1)}, u32[]{:S(2)}, u32[]{:S(2)}) collective-permute-start(bf16[128,128]{1,0:T(8,128)(2,1)} %slice.86), channel_id=1, source_target_pairs={{0,8},{8,16},{16,24},{1,9},{9,17},{17,25},{2,10},{10,18},{18,26},{... | collective-permute-start | bytes 98312 | tf_op jit(solution)/shard_map/ppermute | solution.py:16
  65.8 4.6 %collective-permute-start = (bf16[128,128]{1,0:T(8,128)(2,1)}, bf16[128,128]{1,0:T(8,128)(2,1)S(1)}, u32[]{:S(2)}, u32[]{:S(2)}) collective-permute-start(bf16[128,128]{1,0:T(8,128)(2,1)} %slice.85), channel_id=1, source_target_pairs={{0,8},{8,16},{16,24},{1,9},{9,17},{17,25},{2,10},{10,18},{18,26},{... | collective-permute-start | bytes 98312 | tf_op jit(solution)/shard_map/ppermute | solution.py:16
  81.2 3.4 %copy-start.5 = (bf16[4,128,2,64]{1,3,2,0:T(8,128)(2,1)S(1)}, bf16[4,128,2,64]{1,3,2,0:T(8,128)(2,1)}, u32[]{:S(2)}) copy-start(bf16[4,128,2,64]{1,3,2,0:T(8,128)(2,1)} %copy.41) | copy-start | bytes 393220
  81.2 3.4 %copy-start.6 = (bf16[4,128,2,64]{1,3,2,0:T(8,128)(2,1)S(1)}, bf16[4,128,2,64]{1,3,2,0:T(8,128)(2,1)}, u32[]{:S(2)}) copy-start(bf16[4,128,2,64]{1,3,2,0:T(8,128)(2,1)} %copy.40) | copy-start | bytes 393220
  84.7 39.9 %copy-start.24 = (f32[512]{0:T(512)S(1)}, f32[512]{0:T(512)}, u32[]{:S(2)}) copy-start(f32[512]{0:T(512)} %copy-done.23) | copy-start | bytes 6148
  84.7 39.9 %copy-start.28 = (f32[2048]{0:T(1024)S(1)}, f32[2048]{0:T(1024)}, u32[]{:S(2)}) copy-start(f32[2048]{0:T(1024)} %param.13) | copy-start | bytes 24580
  127.5 0.8 copy-start.2
  128.3 47.2 %copy-start.3 = (bf16[512,512]{1,0:T(8,128)(2,1)S(1)}, bf16[512,512]{1,0:T(8,128)(2,1)}, u32[]{:S(2)}) copy-start(bf16[512,512]{1,0:T(8,128)(2,1)} %copy-done.2) | copy-start | bytes 1572868
  128.3 47.2 %collective-permute-start.2 = (bf16[16,512]{1,0:T(8,128)(2,1)S(1)}, bf16[16,512]{1,0:T(8,128)(2,1)S(1)}, u32[]{:S(2)}, u32[]{:S(2)}) collective-permute-start(bf16[16,512]{1,0:T(8,128)(2,1)S(1)} %slice.87), channel_id=1, source_target_pairs={{0,8},{8,16},{16,24},{1,9},{9,17},{17,25},{2,10},{10,18},{18,26},{... | collective-permute-start | bytes 49160 | tf_op jit(solution)/shard_map/ppermute | solution.py:16
  170.5 5.1 %copy-start.7 = (pred[512]{0:T(512)(128)(4,1)S(1)}, pred[512]{0:T(512)(128)(4,1)}, u32[]{:S(2)}) copy-start(pred[512]{0:T(512)(128)(4,1)} %get-tuple-element.2) | copy-start | bytes 1540
  170.5 5.1 %copy-start.8 = (pred[512]{0:T(512)(128)(4,1)S(1)}, pred[512]{0:T(512)(128)(4,1)}, u32[]{:S(2)}) copy-start(pred[512]{0:T(512)(128)(4,1)} %get-tuple-element.3) | copy-start | bytes 1540
  170.5 5.1 %copy-start.9 = (pred[512]{0:T(512)(128)(4,1)S(1)}, pred[512]{0:T(512)(128)(4,1)}, u32[]{:S(2)}) copy-start(pred[512]{0:T(512)(128)(4,1)} %get-tuple-element.4) | copy-start | bytes 1540
  170.5 5.1 %copy-start.10 = (pred[512]{0:T(512)(128)(4,1)S(1)}, pred[512]{0:T(512)(128)(4,1)}, u32[]{:S(2)}) copy-start(pred[512]{0:T(512)(128)(4,1)} %get-tuple-element.5) | copy-start | bytes 1540
  170.5 5.1 %copy-start.11 = (pred[512]{0:T(512)(128)(4,1)S(1)}, pred[512]{0:T(512)(128)(4,1)}, u32[]{:S(2)}) copy-start(pred[512]{0:T(512)(128)(4,1)} %get-tuple-element.6) | copy-start | bytes 1540
  170.5 5.2 %copy-start.12 = (pred[512]{0:T(512)(128)(4,1)S(1)}, pred[512]{0:T(512)(128)(4,1)}, u32[]{:S(2)}) copy-start(pred[512]{0:T(512)(128)(4,1)} %get-tuple-element.7) | copy-start | bytes 1540
  170.5 5.2 %copy-start.13 = (pred[512]{0:T(512)(128)(4,1)S(1)}, pred[512]{0:T(512)(128)(4,1)}, u32[]{:S(2)}) copy-start(pred[512]{0:T(512)(128)(4,1)} %get-tuple-element.8) | copy-start | bytes 1540
  170.6 5.2 %copy-start.14 = (pred[512]{0:T(512)(128)(4,1)S(1)}, pred[512]{0:T(512)(128)(4,1)}, u32[]{:S(2)}) copy-start(pred[512]{0:T(512)(128)(4,1)} %get-tuple-element.9) | copy-start | bytes 1540
  170.6 5.2 %copy-start.15 = (pred[512]{0:T(512)(128)(4,1)S(1)}, pred[512]{0:T(512)(128)(4,1)}, u32[]{:S(2)}) copy-start(pred[512]{0:T(512)(128)(4,1)} %get-tuple-element.10) | copy-start | bytes 1540
  170.6 5.2 %copy-start.16 = (pred[512]{0:T(512)(128)(4,1)S(1)}, pred[512]{0:T(512)(128)(4,1)}, u32[]{:S(2)}) copy-start(pred[512]{0:T(512)(128)(4,1)} %get-tuple-element.11) | copy-start | bytes 1540
  170.6 5.2 %copy-start.17 = (pred[512]{0:T(512)(128)(4,1)S(1)}, pred[512]{0:T(512)(128)(4,1)}, u32[]{:S(2)}) copy-start(pred[512]{0:T(512)(128)(4,1)} %get-tuple-element.12) | copy-start | bytes 1540
  170.6 5.2 %copy-start.18 = (pred[512]{0:T(512)(128)(4,1)S(1)}, pred[512]{0:T(512)(128)(4,1)}, u32[]{:S(2)}) copy-start(pred[512]{0:T(512)(128)(4,1)} %get-tuple-element.13) | copy-start | bytes 1540
  170.6 5.2 %copy-start.19 = (pred[512]{0:T(512)(128)(4,1)S(1)}, pred[512]{0:T(512)(128)(4,1)}, u32[]{:S(2)}) copy-start(pred[512]{0:T(512)(128)(4,1)} %get-tuple-element.14) | copy-start | bytes 1540
  170.6 5.2 %copy-start.20 = (pred[512]{0:T(512)(128)(4,1)S(1)}, pred[512]{0:T(512)(128)(4,1)}, u32[]{:S(2)}) copy-start(pred[512]{0:T(512)(128)(4,1)} %get-tuple-element.15) | copy-start | bytes 1540
  170.6 5.2 %copy-start.21 = (pred[512]{0:T(512)(128)(4,1)S(1)}, pred[512]{0:T(512)(128)(4,1)}, u32[]{:S(2)}) copy-start(pred[512]{0:T(512)(128)(4,1)} %get-tuple-element.16) | copy-start | bytes 1540
  170.6 5.2 %copy-start.22 = (pred[512]{0:T(512)(128)(4,1)S(1)}, pred[512]{0:T(512)(128)(4,1)}, u32[]{:S(2)}) copy-start(pred[512]{0:T(512)(128)(4,1)} %get-tuple-element.17) | copy-start | bytes 1540
Sparse Core Ops, SparseCore 0:
  9.6 13.2 all-gather.14
  24.5 52.2 all-gather.6
  78.4 46.1 all-gather.10
  126.0 44.4 all-gather.8
  171.9 44.4 all-gather.12
  222.7 10.8 reduce-scatter.1
where the time goes:
time: 244 us; the launch traced here: 243 us
  waiting for transfers between devices  134 us (55%)
  blocking collectives  41 us (17%)
  matrix products  24.4 us (10%)
  between operations  14.6 us (6%)
  other arithmetic  12.1 us (5%)
  local copies, waits for them, and re-layouts  8.64 us (4%)
  starting transfers between devices  8.09 us (3%)
    all_gather x1, waiting for transfers between devices, local(): lax.all_gather(attn_out_weight, 'sp', axis=1, tiled=True)  39.8 us
    all_gather x1, waiting for transfers between devices, local(): lax.all_gather(pool_in_weight, 'sp', axis=0, tiled=True)  38.3 us
    all_gather x1, waiting for transfers between devices, local(): lax.all_gather(pool_out_weight, 'sp', axis=1, tiled=True)  37.1 us
    all_gather x1, blocking collectives, local(): lax.all_gather(value_matrix, 'sp', axis=0, tiled=True)  23.4 us
    all_gather x1, blocking collectives, local(): lax.all_gather(key_matrix, 'sp', axis=0, tiled=True)  17.6 us
    reduce_scatter x1, waiting for transfers between devices, local(): lax.psum_scatter(jnp.dot(attn_part, half_attn, preferred_element_type=jnp...  10.3 us
    dot_general x4, matrix products, local(): jnp.dot(normed, weight, preferred_element_type=jnp.float32)  9.63 us
    ppermute x3, starting transfers between devices, passed_along(): return lax.ppermute(shard, axis, pairs)  7.87 us
  transfers between devices with their start and end apart: 9, of which 6 were waited for; matrix products, arithmetic and copies ran while one was open for 15% of the time, Pallas kernels for 0%

commit v1 on v0

--- a/solution.py
+++ b/solution.py
@@ -152,7 +152,7 @@
     )
     pool_part = pool_branch(pool_rows, pool_tail, mixing, scales, tp_index * groups_dev, first_pos)
     half_attn, half_pool = (
-        lax.all_gather(attn_out_weight, "sp", axis=1, tiled=True),
+        jnp.concatenate(lax.all_gather(attn_out_weight, "sp"), axis=1),
         lax.all_gather(pool_out_weight, "sp", axis=1, tiled=True),
     )
     result = lax.psum_scatter(

time: 244 us -> 244 us (level)
    all_gather x1, waiting for transfers between devices: 38.3 us -> 43.1 us  [local(): lax.all_gather(pool_in_weight, 'sp', axis=0, tiled=True)]
    all_gather x1, waiting for transfers between devices: 37.1 us -> 32.8 us  [local(): lax.all_gather(pool_out_weight, 'sp', axis=1, tiled=True)]
    reshape x0 -> x1, local copies, waits for them, and re-layouts: none -> 2.79 us  [local(): jnp.concatenate(lax.all_gather(attn_out_weight, 'sp'), axis=1)]
where the time goes in v1:
time: 244 us; the launch traced here: 243 us
  waiting for transfers between devices  135 us (55%)
  blocking collectives  41 us (17%)
  matrix products  23.1 us (9%)
  between operations  14.7 us (6%)
  other arithmetic  12.1 us (5%)
  local copies, waits for them, and re-layouts  9.63 us (4%)
  starting transfers between devices  7.97 us (3%)
    all_gather x1, waiting for transfers between devices, local(): lax.all_gather(pool_in_weight, 'sp', axis=0, tiled=True)  43.1 us
    all_gather x1, waiting for transfers between devices, local(): lax.all_gather(attn_out_weight, 'sp')  39.6 us
    all_gather x1, waiting for transfers between devices, local(): lax.all_gather(pool_out_weight, 'sp', axis=1, tiled=True)  32.8 us
    all_gather x1, blocking collectives, local(): lax.all_gather(value_matrix, 'sp', axis=0, tiled=True)  23.4 us
    all_gather x1, blocking collectives, local(): lax.all_gather(key_matrix, 'sp', axis=0, tiled=True)  17.6 us
    reduce_scatter x1, waiting for transfers between devices, local(): lax.psum_scatter(jnp.dot(attn_part, half_attn, preferred_element_type=jnp...  10.3 us
    dot_general x4, matrix products, local(): jnp.dot(normed, weight, preferred_element_type=jnp.float32)  10.3 us
    ppermute x3, starting transfers between devices, passed_along(): return lax.ppermute(shard, axis, pairs)  7.74 us
  transfers between devices with their start and end apart: 9, of which 6 were waited for; matrix products, arithmetic and copies ran while one was open for 15% of the time, Pallas kernels for 0%

profile of v1, /device:TPU:0, one launch (start us, length us, event | category | flops | bytes accessed | tf_op | source)
XLA Modules:
  0.0 243.1 jit_solution(13538314944485270732)
XLA Ops:
  7.2 0.0 all-gather.14.cloned.1.call-start
  7.3 0.7 all-gather.14.cloned.1.call-update
  7.9 0.0 all-gather.8.cloned.1.call-start
  8.0 0.7 all-gather.8.cloned.1.call-update
  8.7 0.0 all-gather.16.cloned.1.call-start
  8.7 0.7 all-gather.16.cloned.1.call-update
  9.4 0.0 all-gather.10.cloned.1.call-start
  9.5 0.5 all-gather.10.cloned.1.call-update
  10.0 0.0 all-gather.12.cloned.1.call-start
  10.1 0.5 all-gather.12.cloned.1.call-update
  10.6 0.0 reduce-scatter.2.cloned.1.call-start
  10.7 0.1 iota_add_fusion
  10.7 0.1 broadcast_compare_fusion
  10.8 17.6 %all_gather.26 = bf16[2048,128]{1,0:T(8,128)(2,1)S(1)} all-gather(bf16[512,128]{1,0:T(8,128)(2,1)} %param.15), channel_id=1, replica_groups=mesh['sp'=4,'fs'=4,'tp'=2] {'sp'}, dimensions={0}, use_global_device_ids=true | all-gather | bytes 655360 | tf_op jit(solution)/shard_map/all_gather | solution.py:115
  28.4 0.7 dynamic_slice.9
  29.1 0.1 max.26
  29.2 23.4 %all_gather.25 = bf16[2048,128]{1,0:T(8,128)(2,1)} all-gather(bf16[512,128]{1,0:T(8,128)(2,1)} %param.16), channel_id=1, replica_groups=mesh['sp'=4,'fs'=4,'tp'=2] {'sp'}, dimensions={0}, use_global_device_ids=true | all-gather | bytes 655360 | tf_op jit(solution)/shard_map/all_gather | solution.py:116
  52.6 0.1 select_reduce_fusion
  52.7 0.6 broadcast_compare_fusion.15
  53.4 0.1 dynamic_slice.11
  53.5 0.3 fusion.36
  53.8 0.0 all-gather.14.cloned.1.call-done
  53.9 2.2 fusion
  56.1 2.4 convolution_convert_fusion.2
  58.5 0.6 slice.86
  59.1 3.5 %collective-permute-start.1 = (bf16[128,128]{1,0:T(8,128)(2,1)}, bf16[128,128]{1,0:T(8,128)(2,1)}, u32[]{:S(2)}, u32[]{:S(2)}) collective-permute-start(bf16[128,128]{1,0:T(8,128)(2,1)} %slice.86), channel_id=1, source_target_pairs={{0,8},{8,16},{16,24},{1,9},{9,17},{17,25},{2,10},{10,18},{18,26},{... | collective-permute-start | bytes 98312 | tf_op jit(solution)/shard_map/ppermute | solution.py:16
  62.6 1.5 convolution_convert_fusion.3
  64.1 0.1 reshape.244
  64.2 0.6 slice.85
  64.8 0.1 reshape.242
  65.0 0.8 copy.61
  65.7 2.0 collective-permute-start
  67.7 0.8 copy.57
  68.5 0.8 pad_maximum_fusion
  69.3 0.1 reshape.243
  69.5 0.8 copy.60
  70.2 0.1 collective-permute-done
  70.3 0.1 reshape.241
  70.5 0.8 copy.56
  71.2 5.6 %all-gather.8.cloned.1.call-done = bf16[2048,512]{1,0:T(8,128)(2,1)} async-done(((bf16[512,512]{1,0:T(8,128)(2,1)}), bf16[2048,512]{1,0:T(8,128)(2,1)}) %all-gather.8.cloned.1.call-update) | async-done | bytes 2097168 | tf_op jit(solution)/shard_map/all_gather | solution.py:114
  76.8 2.9 %convolution_convert_fusion.1 = bf16[512,512]{1,0:T(8,128)(2,1)S(1)} fusion(bf16[2048,512]{1,0:T(8,128)(2,1)} %all-gather.8.cloned.1.call-done, bf16[1,512,2048]{2,1,0:T(8,128)(2,1)S(1)} %copy-done.1, f32[2048]{0:T(1024)} %param.13, f32[512]{0:T(512)} %copy-done.21), kind=kOutput, calls=%fused_computation.13 | convolution fusion | flops 1078198272 | bytes 4728832 | tf_op jit(solution)/shard_map/dot_general | solution.py:123
  79.7 0.5 reshape.245
  80.3 1.9 fusion.4
  82.2 0.1 broadcast_maximum_fusion
  82.3 1.0 fusion.3
  83.3 0.1 exponential_add_fusion
  83.4 1.2 fusion.7
  84.6 0.4 copy.65
  85.0 39.6 %all-gather.16.cloned.1.call-done = bf16[2048,512]{1,0:T(8,128)(2,1)} async-done(((bf16[512,512]{1,0:T(8,128)(2,1)}), bf16[2048,512]{1,0:T(8,128)(2,1)}) %all-gather.16.cloned.1.call-update) | async-done | bytes 2097168 | tf_op jit(solution)/shard_map/all_gather | solution.py:155
  124.6 2.8 %copy.66 = bf16[512,4,512]{0,2,1:T(8,128)(2,1)S(1)} copy(bf16[512,4,512]{2,0,1:T(8,128)(2,1)} %bitcast.81) | data formatting | bytes 4194304 | tf_op jit(solution)/shard_map/reshape | solution.py:155
  127.4 43.1 %all-gather.10.cloned.1.call-done = bf16[2048,512]{1,0:T(8,128)(2,1)} async-done(((bf16[512,512]{1,0:T(8,128)(2,1)}), bf16[2048,512]{1,0:T(8,128)(2,1)}) %all-gather.10.cloned.1.call-update) | async-done | bytes 2097168 | tf_op jit(solution)/shard_map/all_gather | solution.py:117
  170.5 3.5 %convolution_convert_fusion = bf16[512,512]{1,0:T(8,128)(2,1)S(1)} fusion(bf16[2048,512]{1,0:T(8,128)(2,1)} %all-gather.10.cloned.1.call-done, bf16[1,512,2048]{2,1,0:T(8,128)(2,1)} %all-gather.14.cloned.1.call-done, f32[2048]{0:T(1024)S(1)} %copy-done.26, f32[512]{0:T(512)S(1)} %copy-done.22), kind=kOutput, calls=%fused_computation.12 | convolution fusion | flops 1078198272 | bytes 4728832 | tf_op jit(solution)/shard_map/dot_general | solution.py:123
  174.1 2.3 collective-permute-start.2
  176.5 3.3 %fusion.29 = f32[512,2048]{1,0:T(8,128)} fusion(bf16[512,2048]{0,1:T(8,128)(2,1)S(1)} %bitcast.79, bf16[64,8,4,128]{3,2,1,0:T(4,128)(2,1)S(1)} %bitcast.80), kind=kOutput, calls=%fused_computation.59 | convolution fusion | flops 1073741824 | bytes 6815744 | tf_op jit(solution)/shard_map/dot_general | solution.py:159
  179.8 0.1 maximum_convert_fusion
  180.1 3.0 %fusion.28 = bf16[512,512]{1,0:T(8,128)(2,1)S(1)} fusion(f32[528,512]{1,0:T(8,128)S(1)} %maximum_convert_fusion, s32[512]{0:T(512)S(1)} %select_reduce_fusion, s32[512]{0:T(512)S(1)} %add_add_fusion, pred[512]{0:T(512)(128)(4,1)S(1)} %copy-done.6, pred[512]{0:T(512)(128)(4,1)S(1)} %copy-done.7, pred[512]{0:T(512)(128)(4,1)S(1)} %copy-done.8, ...), kind=kLoop, calls=%fused_computation.55 | loop fusion | flops 9437184 | bytes 17313792 | tf_op jit(solution)/shard_map/convert_element_type | solution.py:84
  183.1 0.4 fusion.32
  183.5 0.1 fusion.25
  183.6 32.8 %all-gather.12.cloned.1.call-done = bf16[512,2048]{1,0:T(8,128)(2,1)} async-done(((bf16[512,512]{1,0:T(8,128)(2,1)}), bf16[512,2048]{1,0:T(8,128)(2,1)}) %all-gather.12.cloned.1.call-update) | async-done | bytes 2097168 | tf_op jit(solution)/shard_map/all_gather | solution.py:156
  216.4 6.1 %convolution_add_fusion = f32[512,2048]{1,0:T(8,128)} fusion(f32[512,2048]{1,0:T(8,128)} %fusion.29, bf16[512,512]{0,1:T(8,128)(2,1)S(1)} %fusion.25, bf16[512,2048]{1,0:T(8,128)(2,1)} %all-gather.12.cloned.1.call-done), kind=kOutput, calls=%fused_computation.9 | convolution fusion | flops 1074790400 | bytes 11010048 | tf_op jit(solution)/shard_map/dot_general | solution.py:160
  222.5 0.0 reduce-scatter.2.cloned.1.call-update
  222.5 0.7 fusion.43
  223.2 10.3 %reduce-scatter.2.cloned.1.call-done = f32[256,2048]{1,0:T(8,128)} async-done(((f32[512,2048]{1,0:T(8,128)}), f32[256,2048]{1,0:T(8,128)}) %reduce-scatter.2.cloned.1.call-update) | async-done | bytes 2097168 | tf_op jit(solution)/shard_map/reduce_scatter | solution.py:158
  233.5 2.7 %convert_bitcast_fusion = bf16[1,256,2048]{2,1,0:T(8,128)(2,1)} fusion(f32[256,2048]{1,0:T(8,128)} %reduce-scatter.2.cloned.1.call-done), kind=kLoop, calls=%fused_computation.54 | loop fusion | flops 524288 | bytes 3145728 | tf_op jit(solution)/shard_map/broadcast_in_dim | solution.py:165
  (63 shorter events, 0.2 us)
Async XLA Ops:
  7.2 175.9 %copy-start = (bf16[4,256,256]{2,1,0:T(8,128)(2,1)S(1)}, bf16[4,256,256]{2,1,0:T(8,128)(2,1)}, u32[]{:S(2)}) copy-start(bf16[4,256,256]{2,1,0:T(8,128)(2,1)} %param.19) | copy-start | bytes 1572868
  7.2 45.5 %copy-start.24 = (s32[4]{0:T(128)S(1)}, s32[4]{0:T(128)}, u32[]{:S(2)}) copy-start(s32[4]{0:T(128)} %constant.89.clone) | copy-start | bytes 52
  7.2 46.2 %copy-start.23 = (f32[1024]{0:T(1024)S(1)}, f32[1024]{0:T(1024)}, u32[]{:S(2)}) copy-start(f32[1024]{0:T(1024)} %param.20) | copy-start | bytes 12292
  7.2 48.9 %copy-start.25 = (f32[2048]{0:T(1024)S(1)}, f32[2048]{0:T(1024)}, u32[]{:S(2)}) copy-start(f32[2048]{0:T(1024)} %param.13) | copy-start | bytes 24580
  7.2 46.6 %all-gather.14.cloned.1.call-start = ((), (), s32[]{:S(2)}) async-start(), calls=%async_computation.5 | async-start | bytes 3145728 | tf_op jit(solution)/shard_map/all_gather | solution.py:119
  7.9 68.9 %all-gather.8.cloned.1.call-start = ((), (), s32[]{:S(2)}) async-start(), calls=%async_computation.1 | async-start | bytes 2621440 | tf_op jit(solution)/shard_map/all_gather | solution.py:114
  8.7 115.9 %all-gather.16.cloned.1.call-start = ((), (), s32[]{:S(2)}) async-start(), calls=%async_computation.6 | async-start | bytes 2621440 | tf_op jit(solution)/shard_map/all_gather | solution.py:155
  9.4 161.1 %all-gather.10.cloned.1.call-start = ((), (), s32[]{:S(2)}) async-start(), calls=%async_computation.2 | async-start | bytes 2621440 | tf_op jit(solution)/shard_map/all_gather | solution.py:117
  10.0 206.4 %all-gather.12.cloned.1.call-start = ((), (), s32[]{:S(2)}) async-start(), calls=%async_computation.3 | async-start | bytes 2621440 | tf_op jit(solution)/shard_map/all_gather | solution.py:156
  10.6 222.9 %reduce-scatter.2.cloned.1.call-start = ((), (), s32[]{:S(2)}) async-start(), calls=%async_computation.4 | async-start | bytes 6291456 | tf_op jit(solution)/shard_map/reduce_scatter | solution.py:158
  53.8 8.8 %copy-start.1 = (bf16[1,512,2048]{2,1,0:T(8,128)(2,1)S(1)}, bf16[1,512,2048]{2,1,0:T(8,128)(2,1)}, u32[]{:S(2)}) copy-start(bf16[1,512,2048]{2,1,0:T(8,128)(2,1)} %all-gather.14.cloned.1.call-done) | copy-start | bytes 6291460
  53.8 8.8 %copy-start.2 = (bf16[2048,128]{1,0:T(8,128)(2,1)S(1)}, bf16[2048,128]{1,0:T(8,128)(2,1)}, u32[]{:S(2)}) copy-start(bf16[2048,128]{1,0:T(8,128)(2,1)} %all_gather.25) | copy-start | bytes 1572868
  56.1 6.5 %copy-start.21 = (f32[512]{0:T(512)}, f32[512]{0:T(512)S(1)}, u32[]{:S(2)}) copy-start(f32[512]{0:T(512)S(1)} %add_rsqrt_fusion) | copy-start | bytes 6148
  59.1 9.5 %collective-permute-start.1 = (bf16[128,128]{1,0:T(8,128)(2,1)}, bf16[128,128]{1,0:T(8,128)(2,1)}, u32[]{:S(2)}, u32[]{:S(2)}) collective-permute-start(bf16[128,128]{1,0:T(8,128)(2,1)} %slice.86), channel_id=1, source_target_pairs={{0,8},{8,16},{16,24},{1,9},{9,17},{17,25},{2,10},{10,18},{18,26},{... | collective-permute-start | bytes 98312 | tf_op jit(solution)/shard_map/ppermute | solution.py:16
  65.7 4.6 %collective-permute-start = (bf16[128,128]{1,0:T(8,128)(2,1)}, bf16[128,128]{1,0:T(8,128)(2,1)S(1)}, u32[]{:S(2)}, u32[]{:S(2)}) collective-permute-start(bf16[128,128]{1,0:T(8,128)(2,1)} %slice.85), channel_id=1, source_target_pairs={{0,8},{8,16},{16,24},{1,9},{9,17},{17,25},{2,10},{10,18},{18,26},{... | collective-permute-start | bytes 98312 | tf_op jit(solution)/shard_map/ppermute | solution.py:16
  80.3 3.1 %copy-start.3 = (bf16[4,128,2,64]{1,3,2,0:T(8,128)(2,1)S(1)}, bf16[4,128,2,64]{1,3,2,0:T(8,128)(2,1)}, u32[]{:S(2)}) copy-start(bf16[4,128,2,64]{1,3,2,0:T(8,128)(2,1)} %copy.57) | copy-start | bytes 393220
  80.3 3.1 %copy-start.4 = (bf16[4,128,2,64]{1,3,2,0:T(8,128)(2,1)S(1)}, bf16[4,128,2,64]{1,3,2,0:T(8,128)(2,1)}, u32[]{:S(2)}) copy-start(bf16[4,128,2,64]{1,3,2,0:T(8,128)(2,1)} %copy.56) | copy-start | bytes 393220
  84.6 86.0 %copy-start.22 = (f32[512]{0:T(512)S(1)}, f32[512]{0:T(512)}, u32[]{:S(2)}) copy-start(f32[512]{0:T(512)} %copy-done.21) | copy-start | bytes 6148
  84.6 86.0 %copy-start.26 = (f32[2048]{0:T(1024)S(1)}, f32[2048]{0:T(1024)}, u32[]{:S(2)}) copy-start(f32[2048]{0:T(1024)} %param.13) | copy-start | bytes 24580
  174.1 5.7 %collective-permute-start.2 = (bf16[16,512]{1,0:T(8,128)(2,1)S(1)}, bf16[16,512]{1,0:T(8,128)(2,1)S(1)}, u32[]{:S(2)}, u32[]{:S(2)}) collective-permute-start(bf16[16,512]{1,0:T(8,128)(2,1)S(1)} %slice.87), channel_id=1, source_target_pairs={{0,8},{8,16},{16,24},{1,9},{9,17},{17,25},{2,10},{10,18},{18,26},{... | collective-permute-start | bytes 49160 | tf_op jit(solution)/shard_map/ppermute | solution.py:16
  176.3 3.6 %copy-start.5 = (pred[512]{0:T(512)(128)(4,1)S(1)}, pred[512]{0:T(512)(128)(4,1)}, u32[]{:S(2)}) copy-start(pred[512]{0:T(512)(128)(4,1)} %get-tuple-element.2) | copy-start | bytes 1540
  176.3 3.6 %copy-start.6 = (pred[512]{0:T(512)(128)(4,1)S(1)}, pred[512]{0:T(512)(128)(4,1)}, u32[]{:S(2)}) copy-start(pred[512]{0:T(512)(128)(4,1)} %get-tuple-element.3) | copy-start | bytes 1540
  176.4 3.6 %copy-start.7 = (pred[512]{0:T(512)(128)(4,1)S(1)}, pred[512]{0:T(512)(128)(4,1)}, u32[]{:S(2)}) copy-start(pred[512]{0:T(512)(128)(4,1)} %get-tuple-element.4) | copy-start | bytes 1540
  176.4 3.6 %copy-start.8 = (pred[512]{0:T(512)(128)(4,1)S(1)}, pred[512]{0:T(512)(128)(4,1)}, u32[]{:S(2)}) copy-start(pred[512]{0:T(512)(128)(4,1)} %get-tuple-element.5) | copy-start | bytes 1540
  176.4 3.6 %copy-start.9 = (pred[512]{0:T(512)(128)(4,1)S(1)}, pred[512]{0:T(512)(128)(4,1)}, u32[]{:S(2)}) copy-start(pred[512]{0:T(512)(128)(4,1)} %get-tuple-element.6) | copy-start | bytes 1540
  176.4 3.6 %copy-start.10 = (pred[512]{0:T(512)(128)(4,1)S(1)}, pred[512]{0:T(512)(128)(4,1)}, u32[]{:S(2)}) copy-start(pred[512]{0:T(512)(128)(4,1)} %get-tuple-element.7) | copy-start | bytes 1540
  176.4 3.6 %copy-start.11 = (pred[512]{0:T(512)(128)(4,1)S(1)}, pred[512]{0:T(512)(128)(4,1)}, u32[]{:S(2)}) copy-start(pred[512]{0:T(512)(128)(4,1)} %get-tuple-element.8) | copy-start | bytes 1540
  176.4 3.6 %copy-start.12 = (pred[512]{0:T(512)(128)(4,1)S(1)}, pred[512]{0:T(512)(128)(4,1)}, u32[]{:S(2)}) copy-start(pred[512]{0:T(512)(128)(4,1)} %get-tuple-element.9) | copy-start | bytes 1540
  176.4 3.6 %copy-start.13 = (pred[512]{0:T(512)(128)(4,1)S(1)}, pred[512]{0:T(512)(128)(4,1)}, u32[]{:S(2)}) copy-start(pred[512]{0:T(512)(128)(4,1)} %get-tuple-element.10) | copy-start | bytes 1540
  176.4 3.6 %copy-start.14 = (pred[512]{0:T(512)(128)(4,1)S(1)}, pred[512]{0:T(512)(128)(4,1)}, u32[]{:S(2)}) copy-start(pred[512]{0:T(512)(128)(4,1)} %get-tuple-element.11) | copy-start | bytes 1540
  176.4 3.6 %copy-start.15 = (pred[512]{0:T(512)(128)(4,1)S(1)}, pred[512]{0:T(512)(128)(4,1)}, u32[]{:S(2)}) copy-start(pred[512]{0:T(512)(128)(4,1)} %get-tuple-element.12) | copy-start | bytes 1540
  176.4 3.6 %copy-start.16 = (pred[512]{0:T(512)(128)(4,1)S(1)}, pred[512]{0:T(512)(128)(4,1)}, u32[]{:S(2)}) copy-start(pred[512]{0:T(512)(128)(4,1)} %get-tuple-element.13) | copy-start | bytes 1540
  176.5 3.6 %copy-start.17 = (pred[512]{0:T(512)(128)(4,1)S(1)}, pred[512]{0:T(512)(128)(4,1)}, u32[]{:S(2)}) copy-start(pred[512]{0:T(512)(128)(4,1)} %get-tuple-element.14) | copy-start | bytes 1540
  176.5 3.6 %copy-start.18 = (pred[512]{0:T(512)(128)(4,1)S(1)}, pred[512]{0:T(512)(128)(4,1)}, u32[]{:S(2)}) copy-start(pred[512]{0:T(512)(128)(4,1)} %get-tuple-element.15) | copy-start | bytes 1540
  176.5 3.6 %copy-start.19 = (pred[512]{0:T(512)(128)(4,1)S(1)}, pred[512]{0:T(512)(128)(4,1)}, u32[]{:S(2)}) copy-start(pred[512]{0:T(512)(128)(4,1)} %get-tuple-element.16) | copy-start | bytes 1540
  176.5 3.6 %copy-start.20 = (pred[512]{0:T(512)(128)(4,1)S(1)}, pred[512]{0:T(512)(128)(4,1)}, u32[]{:S(2)}) copy-start(pred[512]{0:T(512)(128)(4,1)} %get-tuple-element.17) | copy-start | bytes 1540
Sparse Core Ops, SparseCore 0:
  9.6 13.2 all-gather.13
  24.5 52.2 all-gather.7
  78.4 46.1 all-gather.15
  126.0 44.4 all-gather.9
  171.9 44.4 all-gather.11
  222.7 10.8 reduce-scatter.1
